TPU v7x, 128 devices: a whole 4x4x4 slice. The times are simulated.
128 devices in a mesh: ep: 32 (over z, y, core), tp: 4 (over x).
Axes of the slice: x: 4, y: 4, z: 4, core: 2. Of those that a mesh axis runs over, the one named last changes fastest.
Arguments:
- query: bfloat16 [32768, 1024], P('ep', 'tp'), may hold values from -6 to 6
- keys: bfloat16 [32768, 1024], P('ep', 'tp'), may hold values from -6 to 6
- values: bfloat16 [32768, 2048], P('ep', 'tp'), may hold values from -6 to 6
- gate_pre: bfloat16 [32768, 2048], P('ep', 'tp'), may hold values from -6 to 6
- log_decay: float32 [16, 32768], P('tp', 'ep'), may hold values from -1 to 0
- out_weight: bfloat16 [2048, 4096], P(None, 'tp'), may hold values from -0.125 to 0.125
- expert_input: bfloat16 [8192, 4096], P(('ep', 'tp')), may hold values from -6 to 6
- norm_gain: float32 [4096], replicated, may hold values from 0.1 to 1.9
- routes: int32 [8192, 2], P(('ep', 'tp')), may hold values from 0 to 31, all different within a row; in each aligned block of 64 rows (0 to 63, 64 to 127, ...) at most 6 rows name the same one
- route_weights: float32 [8192, 2], P(('ep', 'tp')), may hold values from 0.1 to 1
- w_gate: bfloat16 [32, 4096, 1536], P('ep', None, 'tp'), may hold values from -0.09375 to 0.09375
- w_up: bfloat16 [32, 4096, 1536], P('ep', None, 'tp'), may hold values from -0.09375 to 0.09375
- w_down: bfloat16 [32, 1536, 4096], P('ep', 'tp'), may hold values from -0.15625 to 0.15625
Outputs:
- mixed: bfloat16 [32768, 4096], P('ep', 'tp')
- moe_out: bfloat16 [8192, 4096], P(('ep', 'tp'))
Inputs may be any that keep to these rules, and one draw needn't show every extreme that they name: `routes`: each row names 2 different experts; among the rows of one device no expert is named by more than 6 rows, a bound that some block reaches of some device.
All inputs are finite; a program needn't handle non-finite values.
Results may differ from a plain program's by a relative error of at most 0.018.
Values may be sent and summed in bfloat16 or wider, within the bound.
No kernel may reach another device: no remote copies, remote signals or barrier semaphores. Data moves between devices by JAX's collectives and lax.ppermute only.
A program may use at most 128 MiB of HBM per device.

v0:
```python
import jax
import jax.numpy as jnp
from jax import lax
from jax.sharding import Mesh
from jax.sharding import PartitionSpec as P

BLK = 128
EP = ("ep_0", "ep_1", "ep_2")
EP_TP = ("ep_0", "ep_1", "ep_2", "tp")


def filled_with(value, identity):
    return jax.tree.map(
        lambda part, zero: jnp.zeros_like(part) + jnp.asarray(zero, part.dtype), value, identity
    )


def prefix_by_axis(value, axes, combine, identity):
    before = start = filled_with(value, identity)
    subtotal = value
    for axis in reversed(axes):
        count, position = (lax.axis_size(axis), lax.axis_index(axis))
        pieces = jax.tree.map(
            lambda part, kind: lax.all_gather(part.astype(kind), axis),
            subtotal,
            (jnp.bfloat16, jnp.bfloat16),
        )
        inside, subtotal = (start, start)
        for k in range(count):
            passed = k < position
            subtotal = combine(
                subtotal, jax.tree.map(lambda part, own: part[k].astype(own.dtype), pieces, value)
            )
            inside = jax.tree.map(lambda new, old: jnp.where(passed, new, old), subtotal, inside)
        before = combine(inside, before)
    return before


def cut_along(value, dim, count):
    before, after = (value.shape[:dim], value.shape[dim + 1 :])
    return jnp.moveaxis(value.reshape(*before, count, -1, *after), dim, 0)


def laid_out(parts, dim):
    lengths = list(parts.shape[1:])
    lengths[dim] *= parts.shape[0]
    return jnp.moveaxis(parts, 0, dim).reshape(lengths)


def turned_blocks(parts, axes, sequence):
    inside = parts.shape[1:]
    result = parts.reshape(*(lax.axis_size(a) for a in axes), *inside)
    for k in sequence:
        result = lax.all_to_all(result, axes[k], k, k, tiled=True)
    return result.reshape(-1, *inside)


def exchange_by_chip(value, groups, sequence, split_dim, concat_dim):
    count = lax.axis_size(groups[0]) * lax.axis_size(groups[1])
    parts = cut_along(value, split_dim, count)
    return laid_out(turned_blocks(parts, groups, sequence), concat_dim)


def rotate(vectors, position_index):
    half_dim = vectors.shape[-1] // 2
    inverse = 1.0 / 10000.0 ** jnp.linspace(0.0, 1.0, half_dim, dtype=jnp.float32)
    angles = position_index[:, None] * inverse[None, :]
    cosine = jnp.cos(angles)[:, None, :]
    sine_part = jnp.sin(angles)[:, None, :]
    first_half = vectors[..., :half_dim]
    second_half = vectors[..., half_dim:]
    return jnp.concatenate(
        [
            first_half * cosine - second_half * sine_part,
            first_half * sine_part + second_half * cosine,
        ],
        axis=-1,
    )


def retention_block(state, inputs):
    query_blk, key_blk, value_blk, decay_blk = inputs
    width_blk = decay_blk.shape[1]
    running = jnp.cumsum(decay_blk, axis=1)
    spread = running[:, :, None] - running[:, None, :]
    causal = jnp.tril(jnp.ones((width_blk, width_blk), dtype=bool))[None]
    weights = jnp.where(causal, jnp.exp(jnp.where(causal, spread, 0.0)), 0.0)
    scores = jnp.einsum("hid,hjd->hij", query_blk, key_blk) * weights
    output = jnp.einsum("hij,hje->hie", scores, value_blk)
    output = output + jnp.einsum("hid,hde->hie", query_blk * jnp.exp(running)[:, :, None], state)
    closing = running[:, -1:]
    state_next = state * jnp.exp(closing)[:, :, None] + jnp.einsum(
        "hjd,hje->hde", key_blk * jnp.exp(closing - running)[:, :, None], value_blk
    )
    return (state_next, output)


def head_norm(vectors):
    centered = vectors - jnp.mean(vectors, axis=-1, keepdims=True)
    variance = jnp.mean(centered * centered, axis=-1, keepdims=True)
    return centered * lax.rsqrt(variance + 1e-06)


def chain_states(earlier, later):
    return (earlier[0] * later[0], earlier[1] * later[0][:, None, None] + later[1])


def mixer(query, keys, values, gate_pre, log_decay, out_weight):
    rows = query.shape[0]
    heads_here = log_decay.shape[0]
    head_dim = query.shape[1] // heads_here
    value_dim = values.shape[1] // heads_here
    offset = lax.axis_index(EP) * rows
    position_index = (offset + jnp.arange(rows, dtype=jnp.int32)).astype(jnp.float32)
    rotated_q = rotate(
        query.astype(jnp.float32).reshape(rows, heads_here, head_dim), position_index
    )
    rotated_k = rotate(
        keys.astype(jnp.float32).reshape(rows, heads_here, head_dim), position_index
    ) * head_dim ** (-0.5)
    value_rows = values.astype(jnp.float32).reshape(rows, heads_here, value_dim)
    block_count = rows // BLK

    def to_blocks(array):
        return array.reshape(block_count, BLK, heads_here, array.shape[-1]).transpose(0, 2, 1, 3)

    decay_blocks = log_decay.reshape(heads_here, block_count, BLK).transpose(1, 0, 2)
    start_state = jnp.zeros((heads_here, head_dim, value_dim), jnp.float32)
    final_state, outputs = lax.scan(
        retention_block,
        start_state,
        (to_blocks(rotated_q), to_blocks(rotated_k), to_blocks(value_rows), decay_blocks),
    )
    local_out = outputs.transpose(0, 2, 1, 3).reshape(rows, heads_here, value_dim)
    device_factor = jnp.exp(jnp.sum(log_decay, axis=1))
    incoming = prefix_by_axis(
        (device_factor, final_state),
        EP,
        chain_states,
        (jnp.ones((heads_here,), jnp.float32), jnp.zeros_like(final_state)),
    )
    cumulative = jnp.cumsum(log_decay, axis=1)
    reach = jnp.einsum("rhd,hde->rhe", rotated_q * jnp.exp(cumulative.T)[:, :, None], incoming[1])
    combined = local_out + reach
    gate_act = jax.nn.silu(gate_pre.astype(jnp.float32).reshape(rows, heads_here, value_dim))
    gated = (
        (gate_act * head_norm(combined)).reshape(rows, heads_here * value_dim).astype(jnp.bfloat16)
    )
    projected = jnp.dot(
        lax.all_gather(gated, "tp", axis=1, tiled=True),
        out_weight,
        preferred_element_type=jnp.float32,
    )
    return projected.astype(jnp.bfloat16)


def experts(expert_input, norm_gain, routes, route_weights, w_gate, w_up, w_down):
    token_count, width = expert_input.shape
    top_count = routes.shape[1]
    expert_count = lax.axis_size(EP)
    capacity = 3 * token_count * top_count // (2 * expert_count)
    rows_f = expert_input.astype(jnp.float32)
    centered = rows_f - jnp.mean(rows_f, axis=-1, keepdims=True)
    variance = jnp.mean(centered * centered, axis=-1, keepdims=True)
    normed = (centered * lax.rsqrt(variance + 1e-05) * norm_gain).astype(jnp.bfloat16)
    expert_ids = routes.reshape(token_count * top_count)
    expert_hits = (
        expert_ids[:, None] == jnp.arange(expert_count, dtype=jnp.int32)[None, :]
    ).astype(jnp.int32)
    earlier_hits = jnp.cumsum(expert_hits, axis=0) - expert_hits
    slot_index = jnp.sum(earlier_hits * expert_hits, axis=1)
    target = (expert_ids * capacity + slot_index).reshape(token_count, top_count)
    slot_ids = jnp.arange(expert_count * capacity, dtype=jnp.int32)
    placing = jnp.any(target[None, :, :] == slot_ids[:, None, None], axis=2).astype(jnp.bfloat16)
    outbound = jnp.dot(placing, normed, preferred_element_type=jnp.float32).astype(jnp.bfloat16)
    gate_w = w_gate[0]
    up_w = w_up[0]
    down_w = w_down[0]
    arrived = exchange_by_chip(outbound, (("ep_0", "ep_1"), "ep_2"), (1, 0), 0, 0)
    block_rows = lax.all_gather(arrived, "tp", axis=0, tiled=True)
    hidden = (
        jax.nn.silu(jnp.dot(block_rows, gate_w, preferred_element_type=jnp.float32))
        * jnp.dot(block_rows, up_w, preferred_element_type=jnp.float32)
    ).astype(jnp.bfloat16)
    summed = lax.psum_scatter(
        jnp.dot(hidden, down_w, preferred_element_type=jnp.float32).astype(jnp.bfloat16),
        "tp",
        scatter_dimension=0,
        tiled=True,
    )
    returned = lax.all_to_all(summed, EP, split_axis=0, concat_axis=0, tiled=True)
    total = jnp.zeros((token_count, width), jnp.float32)
    for route_index in range(top_count):
        picking = (target[:, route_index][:, None] == slot_ids[None, :]).astype(jnp.bfloat16)
        picked = jnp.dot(picking, returned, preferred_element_type=jnp.float32)
        total = total + route_weights[:, route_index : route_index + 1] * picked
    return total.astype(jnp.bfloat16)


def per_device(
    query,
    keys,
    values,
    gate_pre,
    log_decay,
    out_weight,
    expert_input,
    norm_gain,
    routes,
    route_weights,
    w_gate,
    w_up,
    w_down,
):
    mixed = mixer(query, keys, values, gate_pre, log_decay, out_weight)
    moe_out = experts(expert_input, norm_gain, routes, route_weights, w_gate, w_up, w_down)
    return (mixed, moe_out)


def solution(mesh):
    torus = Mesh(mesh.devices.reshape(4, 4, 2, mesh.shape["tp"]), ("ep_0", "ep_1", "ep_2", "tp"))
    return jax.shard_map(
        per_device,
        mesh=torus,
        in_specs=(
            P(EP, "tp"),
            P(EP, "tp"),
            P(EP, "tp"),
            P(EP, "tp"),
            P("tp", EP),
            P(None, "tp"),
            P(EP_TP, None),
            P(),
            P(EP_TP, None),
            P(EP_TP, None),
            P(EP, None, "tp"),
            P(EP, None, "tp"),
            P(EP, "tp", None),
        ),
        out_specs=(P(EP, "tp"), P(EP_TP, None)),
        check_vma=False,
    )
```

profile of v0, /device:TPU:1, one launch (start us, length us, event | category | flops | bytes accessed | tf_op | source)
XLA Modules:
  0.0 299.7 jit_solution(16685143774155479839)
XLA Ops:
  9.7 1.2 convert_reduce_fusion
  11.0 1.3 fusion.41
  12.3 2.9 convolution_convert_fusion.1
  15.2 3.5 %reshape_reshape.11 = bf16[16,2,6,4096]{3,2,1,0:T(8,128)(2,1)} reshape(bf16[192,4096]{1,0:T(8,128)(2,1)} %convolution_convert_fusion.1) | data formatting | bytes 3145728 | tf_op jit(solution)/shard_map/reshape;reshape | solution.py:52
  18.7 2.5 copy.79
  21.2 6.0 %all_to_all.22 = bf16[16,2,6,4096]{3,0,2,1:T(8,128)(2,1)S(1)} all-to-all(bf16[16,2,6,4096]{3,0,2,1:T(8,128)(2,1)S(1)} %copy.79), channel_id=1, replica_groups=mesh['ep_0'=4,'ep_1'=4,'ep_2'=2,'tp'=4] {'ep_2'}, dimensions={1} | all-to-all | bytes 3145728 | tf_op jit(solution)/shard_map/all_to_all | solution.py:54
  27.2 1.6 copy.80
  28.8 29.6 %all_to_all.23 = bf16[16,2,6,4096]{3,1,2,0:T(2,128)(2,1)S(1)} all-to-all(bf16[16,2,6,4096]{3,1,2,0:T(2,128)(2,1)S(1)} %copy.80), channel_id=1, replica_groups=mesh['ep_0'=4,'ep_1'=4,'ep_2'=2,'tp'=4] {'ep_0','ep_1'}, dimensions={0} | all-to-all | bytes 3145728 | tf_op jit(solution)/shard_map/all_to_all | solution.py:54
  58.4 2.3 copy.81
  60.8 3.7 %reshape_reshape.12 = bf16[192,4096]{1,0:T(8,128)(2,1)} reshape(bf16[16,2,6,4096]{3,2,1,0:T(8,128)(2,1)} %copy.81) | data formatting | bytes 3145728 | tf_op jit(solution)/shard_map/reshape;reshape | solution.py:47
  66.2 3.9 %all-reduce = bf16[8]{0:T(256)(128)(2,1)S(1)} all-reduce(bf16[8]{0:T(256)(128)(2,1)S(1)} %dynamic-update-slice), channel_id=2, replica_groups=mesh['ep_0'=4,'ep_1'=4,'ep_2'=2,'tp'=4] {'ep_2'}, use_global_device_ids=true, to_apply=%add | all-reduce | flops 8 | bytes 32
  70.2 5.5 %all-gather.2 = bf16[4,1,4]{2,1,0:T(2,128)(2,1)S(1)} all-gather(bf16[1,1,4]{2,1,0:T(2,128)(2,1)S(1)} %convert_bitcast_fusion.6), channel_id=1, replica_groups=mesh['ep_0'=4,'ep_1'=4,'ep_2'=2,'tp'=4] {'ep_1'}, dimensions={0}, use_global_device_ids=true | all-gather | bytes 40 | tf_op jit(solution)/shard_map/all_gather | solution.py:24
  75.7 6.7 %all-gather.3 = bf16[4,1,4]{2,1,0:T(2,128)(2,1)S(1)} all-gather(bf16[1,1,4]{2,1,0:T(2,128)(2,1)S(1)} %fusion.132), channel_id=1, replica_groups=mesh['ep_0'=4,'ep_1'=4,'ep_2'=2,'tp'=4] {'ep_0'}, dimensions={0}, use_global_device_ids=true | all-gather | bytes 40 | tf_op jit(solution)/shard_map/all_gather | solution.py:24
  82.3 2.1 copy.69
  84.4 2.2 convert.24
  86.6 2.1 copy.71
  88.6 2.1 convert.25
  91.4 1.9 multiply_subtract_fusion
  93.4 1.2 copy.88
  96.5 2.2 reshape.401
  98.6 2.6 copy.92
  102.3 26.4 %all-gather.9.cloned.1.call-done = bf16[768,4096]{1,0:T(8,128)(2,1)} async-done(((bf16[192,4096]{1,0:T(8,128)(2,1)}), bf16[768,4096]{1,0:T(8,128)(2,1)}) %all-gather.9.cloned.1.call-update) | async-done | bytes 6291472 | tf_op jit(solution)/shard_map/all_gather | solution.py:180
  128.7 6.6 %fusion.31 = f32[768,384]{1,0:T(8,128)S(1)} fusion(bf16[768,4096]{1,0:T(8,128)(2,1)} %all-gather.9.cloned.1.call-done, bf16[1,4096,384]{2,1,0:T(8,128)(2,1)} %param.27), kind=kOutput, calls=%fused_computation.45 | convolution fusion | flops 2415919104 | bytes 10616832 | tf_op jit(solution)/shard_map/dot_general | solution.py:182
  135.3 3.5 %fusion.36 = bf16[768,384]{1,0:T(8,128)(2,1)S(1)} fusion(bf16[768,4096]{1,0:T(8,128)(2,1)S(1)} %copy-done.12, bf16[1,4096,384]{2,1,0:T(8,128)(2,1)S(1)} %copy-done.13, f32[768,384]{1,0:T(8,128)S(1)} %fusion.31), kind=kOutput, calls=%fused_computation.53 | convolution fusion | flops 2417688576 | bytes 11206656 | tf_op jit(solution)/shard_map/dot_general | solution.py:183
  138.8 5.4 %convolution_convert_fusion = bf16[768,4096]{1,0:T(8,128)(2,1)} fusion(bf16[768,384]{1,0:T(8,128)(2,1)S(1)} %fusion.36, bf16[1,384,4096]{2,1,0:T(8,128)(2,1)S(1)} %copy-done), kind=kOutput, calls=%fused_computation.36 | convolution fusion | flops 2419064832 | bytes 10027008 | tf_op jit(solution)/shard_map/dot_general | solution.py:186
  144.3 45.7 %while.13 = (s32[]{:T(128)}, f32[4,64,128]{2,1,0:T(8,128)S(1)}, f32[8,4,128,128]{3,2,1,0:T(8,128)}, f32[8,4,128]{2,1,0:T(4,128)S(1)}, f32[8,4,128,64]{2,0,3,1:T(...) while((s32[]{:T(128)}, f32[4,64,128]{2,1,0:T(8,128)S(1)}, ...), condition=%wide.region_2.4_spmd.clone, body=%wide.region_0.3_spmd.clone.sunk | while | flops 42614784 | bytes 2547404 | solution.py:129
  144.3 1.7 constant_dynamic-slice_fusion.3
  146.4 1.3 fusion.167
  148.9 1.1 convolution_add_fusion.3
  150.0 1.7 constant_dynamic-slice_fusion.3
  152.1 1.3 fusion.167
  154.5 1.1 convolution_add_fusion.3
  155.7 1.8 constant_dynamic-slice_fusion.3
  157.8 1.3 fusion.167
  161.4 1.8 constant_dynamic-slice_fusion.3
  163.5 1.3 fusion.167
  166.0 1.1 convolution_add_fusion.3
  167.1 1.7 constant_dynamic-slice_fusion.3
  169.2 1.3 fusion.167
  172.8 1.7 constant_dynamic-slice_fusion.3
  174.9 1.3 fusion.167
  178.5 1.8 constant_dynamic-slice_fusion.3
  180.7 1.3 fusion.167
  183.2 1.1 convolution_add_fusion.3
  184.3 1.7 constant_dynamic-slice_fusion.3
  186.4 1.3 fusion.167
  188.9 1.1 convolution_add_fusion.3
  190.0 2.0 copy.75
  192.1 1.5 reshape.318
  193.6 1.1 reduce-window.6
  195.2 2.7 copy.68
  197.9 2.2 all-gather.1
  200.3 10.5 %all_gather.37 = bf16[4,4,64,128]{3,2,1,0:T(8,128)(2,1)S(1)} all-gather(bf16[1,4,64,128]{3,2,1,0:T(8,128)(2,1)S(1)} %fusion.78), channel_id=1, replica_groups=mesh['ep_0'=4,'ep_1'=4,'ep_2'=2,'tp'=4] {'ep_1'}, dimensions={0}, use_global_device_ids=true | all-gather | bytes 327680 | tf_op jit(solution)/shard_map/all_gather | solution.py:24
  211.0 9.8 %all_gather.38 = bf16[4,4,64,128]{3,2,1,0:T(8,128)(2,1)S(1)} all-gather(bf16[1,4,64,128]{3,2,1,0:T(8,128)(2,1)S(1)} %fusion.72), channel_id=1, replica_groups=mesh['ep_0'=4,'ep_1'=4,'ep_2'=2,'tp'=4] {'ep_0'}, dimensions={0}, use_global_device_ids=true | all-gather | bytes 327680 | tf_op jit(solution)/shard_map/all_gather | solution.py:24
  220.9 2.3 fusion.138
  223.5 1.3 copy-done.3
  224.8 1.6 multiply_convert_fusion
  226.4 3.5 %all_to_all.16 = bf16[32,6,4096]{2,1,0:T(8,128)(2,1)} reshape(bf16[192,4096]{1,0:T(8,128)(2,1)} %reduce-scatter.2.cloned.1.call-done) | data formatting | bytes 3145728 | tf_op jit(solution)/shard_map/all_to_all | solution.py:191
  229.9 11.2 %all-to-all-start.2 = ((bf16[32,6,4096]{2,1,0:T(8,128)(2,1)}), bf16[32,6,4096]{2,1,0:T(8,128)(2,1)S(1)}, u32[]{:S(2)}, u32[]{:S(2)}) async-start(bf16[32,6,4096]{2,1,0:T(8,128)(2,1)} %all_to_all.16), calls=%async_computation.3 | async-start | bytes 4194304 | tf_op jit(solution)/shard_map/all_to_all | solution.py:191
  241.2 37.9 %all-gather.7.cloned.1.call-done = bf16[1024,2048]{0,1:T(8,128)(2,1)} async-done(((bf16[1024,512]{0,1:T(8,128)(2,1)}), bf16[1024,2048]{0,1:T(8,128)(2,1)}) %all-gather.7.cloned.1.call-update) | async-done | bytes 4194320 | tf_op jit(solution)/shard_map/all_gather | solution.py:150
  279.1 9.4 %convolution_convert_fusion.2 = bf16[1024,1024]{1,0:T(8,128)(2,1)} fusion(bf16[1024,2048]{0,1:T(8,128)(2,1)} %all-gather.7.cloned.1.call-done, bf16[2048,1024]{1,0:T(8,128)(2,1)} %param.22), kind=kOutput, calls=%fused_computation.51 | convolution fusion | flops 4296015872 | bytes 10485760 | tf_op jit(solution)/shard_map/dot_general | solution.py:149
  288.4 1.4 all_to_all.18
  289.9 2.0 convolution_multiply_fusion.2
  291.9 1.3 fusion.27
  (134 shorter events, 24.2 us)
Async XLA Ops:
  7.2 131.6 %copy-start = (bf16[1,384,4096]{2,1,0:T(8,128)(2,1)S(1)}, bf16[1,384,4096]{2,1,0:T(8,128)(2,1)}, u32[]{:S(2)}) copy-start(bf16[1,384,4096]{2,1,0:T(8,128)(2,1)} %param.29) | copy-start | bytes 9437188
  7.2 121.5 %all-gather.9.cloned.1.call-start = ((), (), s32[]{:S(2)}) async-start(), calls=%async_computation.5 | async-start | bytes 7864320 | tf_op jit(solution)/shard_map/all_gather | solution.py:180
  60.8 3.8 %copy-start.14 = (u32[128]{0:T(128)S(1)}, u32[128]{0:T(128)}, u32[]{:S(2)}) copy-start(u32[128]{0:T(128)} %constant.100) | copy-start | bytes 1540
  60.8 5.1 %copy-start.10 = (f32[4,1024]{1,0:T(4,128)S(1)}, f32[4,1024]{1,0:T(4,128)}, u32[]{:S(2)}) copy-start(f32[4,1024]{1,0:T(4,128)} %param.21) | copy-start | bytes 49156
  64.5 161.9 %reduce-scatter.2.cloned.1.call-start = ((), (), s32[]{:S(2)}) async-start(), calls=%async_computation.6 | async-start | bytes 7864320 | tf_op jit(solution)/shard_map/reduce_scatter | solution.py:185
  93.3 1.4 copy-start.4
  93.3 1.4 copy-start.6
  98.6 2.6 copy-start.8
  98.6 2.6 copy-start.9
  128.7 6.6 %copy-start.12 = (bf16[768,4096]{1,0:T(8,128)(2,1)S(1)}, bf16[768,4096]{1,0:T(8,128)(2,1)}, u32[]{:S(2)}) copy-start(bf16[768,4096]{1,0:T(8,128)(2,1)} %all-gather.9.cloned.1.call-done) | copy-start | bytes 18874372
  128.7 6.6 %copy-start.13 = (bf16[1,4096,384]{2,1,0:T(8,128)(2,1)S(1)}, bf16[1,4096,384]{2,1,0:T(8,128)(2,1)}, u32[]{:S(2)}) copy-start(bf16[1,4096,384]{2,1,0:T(8,128)(2,1)} %param.28) | copy-start | bytes 9437188
  144.2 134.8 %all-gather.7.cloned.1.call-start = ((), (), s32[]{:S(2)}) async-start(), calls=%async_computation.4 | async-start | bytes 5242880 | tf_op jit(solution)/shard_map/all_gather | solution.py:150
  195.2 25.7 %copy-start.5 = (f32[1024,4,32]{0,2,1:T(8,128)S(1)}, f32[1024,4,32]{0,2,1:T(8,128)}, u32[]{:S(2)}) copy-start(f32[1024,4,32]{0,2,1:T(8,128)} %copy-done.4) | copy-start | bytes 1572868
  195.2 25.7 %copy-start.7 = (f32[1024,4,32]{0,2,1:T(8,128)S(1)}, f32[1024,4,32]{0,2,1:T(8,128)}, u32[]{:S(2)}) copy-start(f32[1024,4,32]{0,2,1:T(8,128)} %copy-done.6) | copy-start | bytes 1572868
  223.2 1.6 copy-start.3
  229.9 11.2 %copy-start.11 = (f32[64,2]{0,1:T(2,128)S(1)}, f32[64,2]{0,1:T(2,128)}, u32[]{:S(2)}) copy-start(f32[64,2]{0,1:T(2,128)} %param.26) | copy-start | bytes 1540
  229.9 58.5 %all-to-all-start.2 = ((bf16[32,6,4096]{2,1,0:T(8,128)(2,1)}), bf16[32,6,4096]{2,1,0:T(8,128)(2,1)S(1)}, u32[]{:S(2)}, u32[]{:S(2)}) async-start(bf16[32,6,4096]{2,1,0:T(8,128)(2,1)} %all_to_all.16), calls=%async_computation.3 | async-start | bytes 4194304 | tf_op jit(solution)/shard_map/all_to_all | solution.py:191
  289.9 2.0 copy-start.2
  289.9 3.3 %copy-start.1 = (bf16[1,384,4096]{2,1,0:T(8,128)(2,1)S(1)}, bf16[1,384,4096]{2,1,0:T(8,128)(2,1)}, u32[]{:S(2)}) copy-start(bf16[1,384,4096]{2,1,0:T(8,128)(2,1)} %param.29) | copy-start | bytes 9437188
Sparse Core Ops, SparseCore 0:
  64.6 63.9 all-gather.8
  144.3 64.7 reduce-scatter.1
  226.5 52.4 all-gather.6
where the time goes:
time: 301 us; the launch traced here: 300 us
  blocking collectives  74.3 us (25%)
  waiting for transfers between devices  64.3 us (21%)
  matrix products  59.7 us (20%)
  local copies, waits for them, and re-layouts  56.1 us (19%)
  other arithmetic  18.8 us (6%)
  between operations  14.8 us (5%)
  starting transfers between devices  11.3 us (4%)
    all_gather x1, waiting for transfers between devices, mixer(): lax.all_gather(gated, 'tp', axis=1, tiled=True)  37.9 us
    all_to_all x2, blocking collectives, turned_blocks(): result = lax.all_to_all(result, axes[k], k, k, tiled=True)  35.6 us
    all_gather x5, blocking collectives, prefix_by_axis(): lax.all_gather(part.astype(kind), axis)  34.8 us
    all_gather x1, waiting for transfers between devices, experts(): block_rows = lax.all_gather(arrived, 'tp', axis=0, tiled=True)  26.4 us
    dynamic_slice x8, local copies, waits for them, and re-layouts, mixer(): lax.scan(retention_block, start_state, (to_blocks(rotated_q), to_blocks(r...  14.1 us
    all_to_all x1, starting transfers between devices, experts(): lax.all_to_all(summed, EP, split_axis=0, concat_axis=0, tiled=True)  11.2 us
    unnamed x40, local copies, waits for them, and re-layouts  10.2 us
    dot_general x8, matrix products, retention_block(): output = jnp.einsum('hij,hje->hie', scores, value_blk)  10.2 us
  transfers between devices with their start and end apart: 4, of which 2 were waited for; matrix products, arithmetic and copies ran while one was open for 29% of the time, Pallas kernels for 0%

commit v1 on v0

--- a/solution.py
+++ b/solution.py
@@ -177,7 +177,10 @@
     up_w = w_up[0]
     down_w = w_down[0]
     arrived = exchange_by_chip(outbound, (("ep_0", "ep_1"), "ep_2"), (1, 0), 0, 0)
-    block_rows = lax.all_gather(arrived, "tp", axis=0, tiled=True)
+    devices = lax.axis_size("tp")
+    shards = jnp.stack([arrived for _ in range(devices)])
+    shards = lax.all_to_all(shards, "tp", split_axis=0, concat_axis=0)
+    block_rows = jnp.concatenate(shards, axis=0)
     hidden = (
         jax.nn.silu(jnp.dot(block_rows, gate_w, preferred_element_type=jnp.float32))
         * jnp.dot(block_rows, up_w, preferred_element_type=jnp.float32)

time: 301 us -> 318 us (1.056)
  local copies, waits for them, and re-layouts: 56.1 us -> 60.9 us
  starting transfers between devices: 11.3 us -> 15.5 us
    all_to_all x0 -> x1, waiting for transfers between devices: none -> 30.8 us  [experts(): shards = lax.all_to_all(shards, 'tp', split_axis=0, concat_axis=0)]
    all_gather x1 -> x0, waiting for transfers between devices: 26.4 us -> none  [experts(): block_rows = lax.all_gather(arrived, 'tp', axis=0, tiled=True)]
    all_to_all x0 -> x1, starting transfers between devices: none -> 5.36 us  [experts(): shards = lax.all_to_all(shards, 'tp', split_axis=0, concat_axis=0)]
    another operation x1 -> x2, local copies, waits for them, and re-layouts: 3.71 us -> 8.51 us  [experts(): shards = jnp.stack([arrived for _ in range(devices)])]
    unnamed x40 -> x38, local copies, waits for them, and re-layouts: 10.2 us -> 10.2 us
  transfers between devices with their start and end apart: 4 -> 4, of which waited for: 2 -> 2; matrix products, arithmetic and copies ran while one was open for 29% -> 28% of each run, Pallas kernels for 0% -> 0%
where the time goes in v1:
time: 318 us; the launch traced here: 316 us
  blocking collectives  76.3 us (24%)
  waiting for transfers between devices  67.1 us (21%)
  matrix products  62.4 us (20%)
  local copies, waits for them, and re-layouts  60.9 us (19%)
  other arithmetic  18.7 us (6%)
  starting transfers between devices  15.5 us (5%)
  between operations  15.1 us (5%)
    all_gather x5, blocking collectives, prefix_by_axis(): lax.all_gather(part.astype(kind), axis)  36.8 us
    all_gather x1, waiting for transfers between devices, mixer(): lax.all_gather(gated, 'tp', axis=1, tiled=True)  36.2 us
    all_to_all x2, blocking collectives, turned_blocks(): result = lax.all_to_all(result, axes[k], k, k, tiled=True)  35.6 us
    all_to_all x1, waiting for transfers between devices, experts(): shards = lax.all_to_all(shards, 'tp', split_axis=0, concat_axis=0)  30.8 us
    dynamic_slice x8, local copies, waits for them, and re-layouts, mixer(): lax.scan(retention_block, start_state, (to_blocks(rotated_q), to_blocks(r...  14.2 us
    unnamed x38, local copies, waits for them, and re-layouts  10.2 us
    dot_general x8, matrix products, retention_block(): output = jnp.einsum('hij,hje->hie', scores, value_blk)  10.2 us
    all_to_all x1, starting transfers between devices, experts(): lax.all_to_all(summed, EP, split_axis=0, concat_axis=0, tiled=True)  10.1 us
  transfers between devices with their start and end apart: 4, of which 2 were waited for; matrix products, arithmetic and copies ran while one was open for 28% of the time, Pallas kernels for 0%

profile of v1, /device:TPU:1, one launch (start us, length us, event | category | flops | bytes accessed | tf_op | source)
XLA Modules:
  0.0 316.4 jit_solution(6342259772320767318)
XLA Ops:
  9.7 1.2 convert_reduce_fusion
  10.9 1.3 fusion.41
  12.3 2.9 convolution_convert_fusion.1
  15.2 3.5 %reshape_reshape.8 = bf16[16,2,6,4096]{3,2,1,0:T(8,128)(2,1)} reshape(bf16[192,4096]{1,0:T(8,128)(2,1)} %convolution_convert_fusion.1) | data formatting | bytes 3145728 | tf_op jit(solution)/shard_map/reshape;reshape | solution.py:52
  18.6 2.5 copy.79
  21.1 6.0 %all_to_all.27 = bf16[16,2,6,4096]{3,0,2,1:T(8,128)(2,1)S(1)} all-to-all(bf16[16,2,6,4096]{3,0,2,1:T(8,128)(2,1)S(1)} %copy.79), channel_id=1, replica_groups=mesh['ep_0'=4,'ep_1'=4,'ep_2'=2,'tp'=4] {'ep_2'}, dimensions={1} | all-to-all | bytes 3145728 | tf_op jit(solution)/shard_map/all_to_all | solution.py:54
  27.1 1.6 copy.80
  28.7 29.6 %all_to_all.28 = bf16[16,2,6,4096]{3,1,2,0:T(2,128)(2,1)S(1)} all-to-all(bf16[16,2,6,4096]{3,1,2,0:T(2,128)(2,1)S(1)} %copy.80), channel_id=1, replica_groups=mesh['ep_0'=4,'ep_1'=4,'ep_2'=2,'tp'=4] {'ep_0','ep_1'}, dimensions={0} | all-to-all | bytes 3145728 | tf_op jit(solution)/shard_map/all_to_all | solution.py:54
  58.4 2.3 copy.81
  60.7 3.7 %stack_reshape_reshape.2 = bf16[192,4096]{1,0:T(8,128)(2,1)} reshape(bf16[16,2,6,4096]{3,2,1,0:T(8,128)(2,1)} %copy.81) | data formatting | bytes 3145728 | tf_op jit(solution)/shard_map/stack;reshape;reshape | solution.py:181
  64.4 4.9 %stack.3 = bf16[4,192,4096]{2,1,0:T(8,128)(2,1)} broadcast(bf16[192,4096]{1,0:T(8,128)(2,1)} %stack_reshape_reshape.2), dimensions={1,2} | broadcast | bytes 7864320 | tf_op jit(solution)/shard_map/stack | solution.py:181
  69.2 5.4 %all-to-all-start.2 = ((bf16[4,192,4096]{2,1,0:T(8,128)(2,1)}), bf16[4,192,4096]{2,1,0:T(8,128)(2,1)}, u32[]{:S(2)}, u32[]{:S(2)}) async-start(bf16[4,192,4096]{2,1,0:T(8,128)(2,1)} %stack.3), calls=%async_computation.2 | async-start | bytes 12582912 | tf_op jit(solution)/shard_map/all_to_all | solution.py:182
  76.3 3.9 %all-reduce = bf16[8]{0:T(256)(128)(2,1)S(1)} all-reduce(bf16[8]{0:T(256)(128)(2,1)S(1)} %dynamic-update-slice), channel_id=2, replica_groups=mesh['ep_0'=4,'ep_1'=4,'ep_2'=2,'tp'=4] {'ep_2'}, use_global_device_ids=true, to_apply=%add | all-reduce | flops 8 | bytes 32
  80.2 6.3 %all-gather.2 = bf16[4,1,4]{2,1,0:T(2,128)(2,1)S(1)} all-gather(bf16[1,1,4]{2,1,0:T(2,128)(2,1)S(1)} %convert_bitcast_fusion.6), channel_id=1, replica_groups=mesh['ep_0'=4,'ep_1'=4,'ep_2'=2,'tp'=4] {'ep_1'}, dimensions={0}, use_global_device_ids=true | all-gather | bytes 40 | tf_op jit(solution)/shard_map/all_gather | solution.py:24
  86.6 7.1 %all-gather.3 = bf16[4,1,4]{2,1,0:T(2,128)(2,1)S(1)} all-gather(bf16[1,1,4]{2,1,0:T(2,128)(2,1)S(1)} %fusion.132), channel_id=1, replica_groups=mesh['ep_0'=4,'ep_1'=4,'ep_2'=2,'tp'=4] {'ep_0'}, dimensions={0}, use_global_device_ids=true | all-gather | bytes 40 | tf_op jit(solution)/shard_map/all_gather | solution.py:24
  93.6 2.0 copy.69
  95.7 2.1 convert.24
  97.8 2.0 copy.71
  99.8 2.2 convert.25
  102.7 1.8 multiply_subtract_fusion
  104.7 1.3 copy.88
  107.7 2.1 reshape.407
  109.8 2.5 copy.92
  113.4 30.8 %all-to-all-done.2 = bf16[4,192,4096]{2,1,0:T(8,128)(2,1)} async-done(((bf16[4,192,4096]{2,1,0:T(8,128)(2,1)}), bf16[4,192,4096]{2,1,0:T(8,128)(2,1)}, u32[]{:S(2)}, u32[]{:S(2)}) %all-to-all-start.2) | async-done | bytes 6291488 | tf_op jit(solution)/shard_map/all_to_all | solution.py:182
  144.3 6.6 %fusion.31 = f32[768,384]{1,0:T(8,128)S(1)} fusion(bf16[768,4096]{1,0:T(8,128)(2,1)} %bitcast.41, bf16[1,4096,384]{2,1,0:T(8,128)(2,1)} %param.27), kind=kOutput, calls=%fused_computation.45 | convolution fusion | flops 2415919104 | bytes 10616832 | tf_op jit(solution)/shard_map/dot_general | solution.py:185
  150.9 6.3 %fusion.36 = bf16[768,384]{1,0:T(8,128)(2,1)S(1)} fusion(bf16[768,4096]{1,0:T(8,128)(2,1)} %bitcast.41, bf16[1,4096,384]{2,1,0:T(8,128)(2,1)S(1)} %copy-done.12, f32[768,384]{1,0:T(8,128)S(1)} %fusion.31), kind=kOutput, calls=%fused_computation.53 | convolution fusion | flops 2417688576 | bytes 11206656 | tf_op jit(solution)/shard_map/dot_general | solution.py:186
  157.1 5.3 %convolution_convert_fusion = bf16[768,4096]{1,0:T(8,128)(2,1)} fusion(bf16[768,384]{1,0:T(8,128)(2,1)S(1)} %fusion.36, bf16[1,384,4096]{2,1,0:T(8,128)(2,1)S(1)} %copy-done), kind=kOutput, calls=%fused_computation.36 | convolution fusion | flops 2419064832 | bytes 10027008 | tf_op jit(solution)/shard_map/dot_general | solution.py:189
  162.5 45.8 %while.13 = (s32[]{:T(128)}, f32[4,64,128]{2,1,0:T(8,128)S(1)}, f32[8,4,128,128]{3,2,1,0:T(8,128)}, f32[8,4,128]{2,1,0:T(4,128)S(1)}, f32[8,4,128,64]{2,0,3,1:T(...) while((s32[]{:T(128)}, f32[4,64,128]{2,1,0:T(8,128)S(1)}, ...), condition=%wide.region_2.4_spmd.clone, body=%wide.region_0.3_spmd.clone.sunk | while | flops 42614784 | bytes 2547404 | solution.py:129
  162.5 1.7 constant_dynamic-slice_fusion.3
  164.6 1.3 fusion.167
  168.2 1.9 constant_dynamic-slice_fusion.3
  170.5 1.3 fusion.167
  173.0 1.1 convolution_add_fusion.3
  174.1 1.7 constant_dynamic-slice_fusion.3
  176.2 1.3 fusion.167
  179.8 1.7 constant_dynamic-slice_fusion.3
  181.9 1.3 fusion.167
  185.5 1.8 constant_dynamic-slice_fusion.3
  187.6 1.3 fusion.167
  190.1 1.1 convolution_add_fusion.3
  191.2 1.7 constant_dynamic-slice_fusion.3
  193.3 1.3 fusion.167
  196.9 1.7 constant_dynamic-slice_fusion.3
  199.0 1.3 fusion.167
  202.6 1.8 constant_dynamic-slice_fusion.3
  204.8 1.3 fusion.167
  207.3 1.1 convolution_add_fusion.3
  208.4 2.0 copy.75
  210.4 1.5 reshape.323
  212.0 1.1 reduce-window.6
  213.6 2.7 copy.68
  216.2 4.4 %all-gather.1 = bf16[8,64,128]{2,1,0:T(8,128)(2,1)S(1)} all-gather(bf16[4,64,128]{2,1,0:T(8,128)(2,1)S(1)} %convert_element_type.310), channel_id=3, replica_groups=mesh['ep_0'=4,'ep_1'=4,'ep_2'=2,'tp'=4] {'ep_2'}, dimensions={0}, use_global_device_ids=true | all-gather | bytes 196608 | tf_op jit(solution)/shard_map/all_gather | solution.py:24
  220.8 9.4 %all_gather.34 = bf16[4,4,64,128]{3,2,1,0:T(8,128)(2,1)S(1)} all-gather(bf16[1,4,64,128]{3,2,1,0:T(8,128)(2,1)S(1)} %fusion.78), channel_id=1, replica_groups=mesh['ep_0'=4,'ep_1'=4,'ep_2'=2,'tp'=4] {'ep_1'}, dimensions={0}, use_global_device_ids=true | all-gather | bytes 327680 | tf_op jit(solution)/shard_map/all_gather | solution.py:24
  230.3 9.7 %all_gather.35 = bf16[4,4,64,128]{3,2,1,0:T(8,128)(2,1)S(1)} all-gather(bf16[1,4,64,128]{3,2,1,0:T(8,128)(2,1)S(1)} %fusion.72), channel_id=1, replica_groups=mesh['ep_0'=4,'ep_1'=4,'ep_2'=2,'tp'=4] {'ep_0'}, dimensions={0}, use_global_device_ids=true | all-gather | bytes 327680 | tf_op jit(solution)/shard_map/all_gather | solution.py:24
  240.0 2.3 fusion.138
  242.7 1.3 copy-done.3
  243.9 1.6 multiply_convert_fusion
  245.6 3.5 %all_to_all.20 = bf16[32,6,4096]{2,1,0:T(8,128)(2,1)} reshape(bf16[192,4096]{1,0:T(8,128)(2,1)} %reduce-scatter.2.cloned.1.call-done) | data formatting | bytes 3145728 | tf_op jit(solution)/shard_map/all_to_all | solution.py:194
  249.1 10.1 %all-to-all-start.3 = ((bf16[32,6,4096]{2,1,0:T(8,128)(2,1)}), bf16[32,6,4096]{2,1,0:T(8,128)(2,1)S(1)}, u32[]{:S(2)}, u32[]{:S(2)}) async-start(bf16[32,6,4096]{2,1,0:T(8,128)(2,1)} %all_to_all.20), calls=%async_computation.4 | async-start | bytes 4194304 | tf_op jit(solution)/shard_map/all_to_all | solution.py:194
  259.2 36.2 %all-gather.6.cloned.1.call-done = bf16[1024,2048]{0,1:T(8,128)(2,1)} async-done(((bf16[1024,512]{0,1:T(8,128)(2,1)}), bf16[1024,2048]{0,1:T(8,128)(2,1)}) %all-gather.6.cloned.1.call-update) | async-done | bytes 4194320 | tf_op jit(solution)/shard_map/all_gather | solution.py:150
  295.4 9.4 %convolution_convert_fusion.2 = bf16[1024,1024]{1,0:T(8,128)(2,1)} fusion(bf16[1024,2048]{0,1:T(8,128)(2,1)} %all-gather.6.cloned.1.call-done, bf16[2048,1024]{1,0:T(8,128)(2,1)} %param.22), kind=kOutput, calls=%fused_computation.51 | convolution fusion | flops 4296015872 | bytes 10485760 | tf_op jit(solution)/shard_map/dot_general | solution.py:149
  304.8 1.4 all_to_all.22
  306.2 2.0 convolution_multiply_fusion.2
  308.3 1.3 fusion.27
  (132 shorter events, 26.2 us)
Async XLA Ops:
  7.2 150.0 %copy-start = (bf16[1,384,4096]{2,1,0:T(8,128)(2,1)S(1)}, bf16[1,384,4096]{2,1,0:T(8,128)(2,1)}, u32[]{:S(2)}) copy-start(bf16[1,384,4096]{2,1,0:T(8,128)(2,1)} %param.29) | copy-start | bytes 9437188
  69.2 5.4 %copy-start.13 = (u32[128]{0:T(128)S(1)}, u32[128]{0:T(128)}, u32[]{:S(2)}) copy-start(u32[128]{0:T(128)} %constant.100) | copy-start | bytes 1540
  69.2 6.7 %copy-start.10 = (f32[4,1024]{1,0:T(4,128)S(1)}, f32[4,1024]{1,0:T(4,128)}, u32[]{:S(2)}) copy-start(f32[4,1024]{1,0:T(4,128)} %param.21) | copy-start | bytes 49156
  69.2 75.0 %all-to-all-start.2 = ((bf16[4,192,4096]{2,1,0:T(8,128)(2,1)}), bf16[4,192,4096]{2,1,0:T(8,128)(2,1)}, u32[]{:S(2)}, u32[]{:S(2)}) async-start(bf16[4,192,4096]{2,1,0:T(8,128)(2,1)} %stack.3), calls=%async_computation.2 | async-start | bytes 12582912 | tf_op jit(solution)/shard_map/all_to_all | solution.py:182
  74.6 171.0 %reduce-scatter.2.cloned.1.call-start = ((), (), s32[]{:S(2)}) async-start(), calls=%async_computation.6 | async-start | bytes 7864320 | tf_op jit(solution)/shard_map/reduce_scatter | solution.py:188
  104.5 1.4 copy-start.4
  104.5 1.4 copy-start.6
  109.8 2.6 copy-start.8
  109.8 2.6 copy-start.9
  144.3 6.6 %copy-start.12 = (bf16[1,4096,384]{2,1,0:T(8,128)(2,1)S(1)}, bf16[1,4096,384]{2,1,0:T(8,128)(2,1)}, u32[]{:S(2)}) copy-start(bf16[1,4096,384]{2,1,0:T(8,128)(2,1)} %param.28) | copy-start | bytes 9437188
  162.5 133.0 %all-gather.6.cloned.1.call-start = ((), (), s32[]{:S(2)}) async-start(), calls=%async_computation.5 | async-start | bytes 5242880 | tf_op jit(solution)/shard_map/all_gather | solution.py:150
  213.5 26.5 %copy-start.5 = (f32[1024,4,32]{0,2,1:T(8,128)S(1)}, f32[1024,4,32]{0,2,1:T(8,128)}, u32[]{:S(2)}) copy-start(f32[1024,4,32]{0,2,1:T(8,128)} %copy-done.4) | copy-start | bytes 1572868
  213.5 26.5 %copy-start.7 = (f32[1024,4,32]{0,2,1:T(8,128)S(1)}, f32[1024,4,32]{0,2,1:T(8,128)}, u32[]{:S(2)}) copy-start(f32[1024,4,32]{0,2,1:T(8,128)} %copy-done.6) | copy-start | bytes 1572868
  242.3 1.6 copy-start.3
  249.1 10.1 %copy-start.11 = (f32[64,2]{0,1:T(2,128)S(1)}, f32[64,2]{0,1:T(2,128)}, u32[]{:S(2)}) copy-start(f32[64,2]{0,1:T(2,128)} %param.26) | copy-start | bytes 1540
  249.1 55.7 %all-to-all-start.3 = ((bf16[32,6,4096]{2,1,0:T(8,128)(2,1)}), bf16[32,6,4096]{2,1,0:T(8,128)(2,1)S(1)}, u32[]{:S(2)}, u32[]{:S(2)}) async-start(bf16[32,6,4096]{2,1,0:T(8,128)(2,1)} %all_to_all.20), calls=%async_computation.4 | async-start | bytes 4194304 | tf_op jit(solution)/shard_map/all_to_all | solution.py:194
  306.2 2.0 copy-start.2
  306.2 3.3 %copy-start.1 = (bf16[1,384,4096]{2,1,0:T(8,128)(2,1)S(1)}, bf16[1,384,4096]{2,1,0:T(8,128)(2,1)}, u32[]{:S(2)}) copy-start(bf16[1,384,4096]{2,1,0:T(8,128)(2,1)} %param.29) | copy-start | bytes 9437188
Sparse Core Ops, SparseCore 0:
  162.6 62.0 reduce-scatter.1
  245.7 49.7 all-gather.5
